TPU v7x, 32 devices: a whole 2x2x4 slice. The times are simulated.
32 devices in a mesh: sp: 8 (over z, x), dp: 4 (over y, core).
Axes of the slice: x: 2, y: 2, z: 4, core: 2. Of those that a mesh axis runs over, the one named last changes fastest.
Arguments:
- resid: bfloat16 [4, 2048, 2048], P('dp', 'sp'), may hold values from -4 to 4
- query: bfloat16 [4, 2048, 2048], P('dp', 'sp'), may hold values from -6 to 6
- keys: bfloat16 [4, 2048, 512], P('dp', 'sp'), may hold values from -6 to 6
- values: bfloat16 [4, 2048, 512], P('dp', 'sp'), may hold values from -6 to 6
- q_gain: float32 [128], replicated, may hold values from 0.7 to 5
- k_gain: float32 [128], replicated, may hold values from 0.7 to 5
- out_weight: bfloat16 [2048, 2048], P('dp'), may hold values from -0.5 to 0.5
- norm_gain: float32 [2048], replicated, may hold values from 0.1 to 1.9
- route_ids: int32 [4, 2048, 2], P('dp', 'sp'), may hold values from 0 to 31, all different within a row; in each aligned block of 256 rows (0 to 255, 256 to 511, ..., all dimensions but the last counted through in order) at most 24 rows name the same one
- route_weight: float32 [4, 2048, 2], P('dp', 'sp'), may hold values from 0.2 to 1
- expert_gate: bfloat16 [32, 2048, 1024], P(('sp', 'dp')), may hold values from -0.125 to 0.125
- expert_up: bfloat16 [32, 2048, 1024], P(('sp', 'dp')), may hold values from -0.125 to 0.125
- expert_down: bfloat16 [32, 1024, 2048], P(('sp', 'dp')), may hold values from -0.1875 to 0.1875
Outputs:
- layer_out: bfloat16 [4, 2048, 2048], P('dp', 'sp')
Inputs may be any that keep to these rules, and one draw needn't show every extreme that they name: `route_ids`: each row names 2 different experts. In the rows of one device no expert is named more than 24 times, and in some devices some expert is named exactly 24 times.
All inputs are finite; a program needn't handle non-finite values.
Results may differ from a plain program's by a relative error of at most 0.0095.
The roundings to bfloat16 on the way count: a program that leaves them out, or rounds other values in their place, can miss the bound.
Values may be sent and summed in bfloat16 or wider, within the bound.
A program may use at most 128 MiB of HBM per device.

v0:
```python
import jax
import jax.numpy as jnp
from jax import lax
from jax.sharding import PartitionSpec as P

GRID_W = 64
EPSILON = 1e-06
THETA = 10000.0
LIMIT = 7.0
SLOPE = 1.702


def turn_half(matrix, places):
    half_width = matrix.shape[-1] // 2
    inverse = THETA ** (-jnp.arange(half_width, dtype=jnp.float32) / half_width)
    angles = places.astype(jnp.float32)[:, None] * inverse[None, :]
    cosine = jnp.cos(angles)[:, None, :]
    sine_part = jnp.sin(angles)[:, None, :]
    leading = matrix[..., :half_width]
    second = matrix[..., half_width:]
    return jnp.concatenate(
        [leading * cosine - second * sine_part, second * cosine + leading * sine_part], axis=-1
    )


def prepare(projected_rows, gain_vector, head_count, places):
    matrix = projected_rows.astype(jnp.float32).reshape(projected_rows.shape[0], head_count, -1)
    matrix = (
        matrix
        * lax.rsqrt(jnp.mean(matrix * matrix, axis=-1, keepdims=True) + EPSILON)
        * gain_vector
    )
    middle = matrix.shape[-1] // 2
    turned = jnp.concatenate(
        [
            turn_half(matrix[..., :middle], places // GRID_W),
            turn_half(matrix[..., middle:], places % GRID_W),
        ],
        axis=-1,
    )
    return turned.astype(jnp.bfloat16)


def attend(head_query, head_key, head_value):
    length, local_heads, head_dim = head_query.shape
    local_kv = head_key.shape[1]
    group_size = local_heads // local_kv
    block_rows = min(512, length)
    scaling = head_dim ** (-0.5)
    query_blocks = head_query.reshape(
        length // block_rows, block_rows, local_kv, group_size, head_dim
    )

    def one_block(query_block):
        scores = (
            jnp.einsum("qkgd,skd->kgqs", query_block, head_key, preferred_element_type=jnp.float32)
            * scaling
        )
        lifted = jnp.exp(scores - jnp.max(scores, axis=-1, keepdims=True))
        attn_weights = (lifted / jnp.sum(lifted, axis=-1, keepdims=True)).astype(jnp.bfloat16)
        return jnp.einsum(
            "kgqs,skd->qkgd", attn_weights, head_value, preferred_element_type=jnp.float32
        ).astype(jnp.bfloat16)

    return lax.map(one_block, query_blocks).reshape(length, local_heads, head_dim)


def apply_expert(batch, gate_matrix, up_matrix, down_matrix):
    flat_rows = batch.reshape(-1, batch.shape[-1])
    gated = jnp.minimum(jnp.dot(flat_rows, gate_matrix, preferred_element_type=jnp.float32), LIMIT)
    linear = jnp.clip(
        jnp.dot(flat_rows, up_matrix, preferred_element_type=jnp.float32), -LIMIT, LIMIT
    )
    active = (gated * jax.nn.sigmoid(SLOPE * gated) * (linear + 1.0)).astype(jnp.bfloat16)
    return (
        jnp.dot(active, down_matrix, preferred_element_type=jnp.float32)
        .astype(jnp.bfloat16)
        .reshape(batch.shape)
    )


def per_device(
    resid,
    query,
    keys,
    values,
    q_gain,
    k_gain,
    out_weight,
    norm_gain,
    route_ids,
    route_weight,
    expert_gate,
    expert_up,
    expert_down,
):
    span_devices = lax.axis_size("sp")
    experts_total = span_devices * lax.axis_size("dp")
    tok_rows = resid.shape[1]
    model_width = resid.shape[2]
    head_dim = q_gain.shape[0]
    q_heads = query.shape[2] // head_dim
    kv_heads = keys.shape[2] // head_dim
    repeat_count = max(kv_heads, span_devices) // kv_heads
    places = lax.axis_index("sp") * tok_rows + jnp.arange(tok_rows, dtype=jnp.int32)
    query_turned = prepare(query[0], q_gain, q_heads, places)
    key_turned = jnp.repeat(prepare(keys[0], k_gain, kv_heads, places), repeat_count, axis=1)
    value_heads = jnp.repeat(values[0].reshape(tok_rows, kv_heads, head_dim), repeat_count, axis=1)
    head_query, head_key, head_value = (
        lax.all_to_all(query_turned, "sp", split_axis=1, concat_axis=0, tiled=True),
        lax.all_to_all(key_turned, "sp", split_axis=1, concat_axis=0, tiled=True),
        lax.all_to_all(value_heads, "sp", split_axis=1, concat_axis=0, tiled=True),
    )
    head_out = attend(head_query, head_key, head_value)
    token_out = lax.all_to_all(head_out, "sp", split_axis=0, concat_axis=1, tiled=True).reshape(
        tok_rows, q_heads * head_dim
    )
    projected = jnp.dot(
        token_out,
        lax.all_gather(out_weight, "dp", axis=0, tiled=True),
        preferred_element_type=jnp.float32,
    )
    updated = (resid[0].astype(jnp.float32) + projected).astype(jnp.bfloat16)
    widened = updated.astype(jnp.float32)
    normed = (
        widened
        * lax.rsqrt(jnp.mean(widened * widened, axis=-1, keepdims=True) + EPSILON)
        * norm_gain
    ).astype(jnp.bfloat16)
    top_count = route_ids.shape[2]
    capacity = max(2, 3 * tok_rows * top_count // (2 * experts_total))
    chosen = route_ids[0].reshape(-1)
    onehot = (chosen[:, None] == jnp.arange(experts_total, dtype=jnp.int32)[None, :]).astype(
        jnp.int32
    )
    earlier = jnp.sum((jnp.cumsum(onehot, axis=0) - onehot) * onehot, axis=1)
    target = chosen * capacity + earlier
    sources = jnp.arange(tok_rows * top_count, dtype=jnp.int32) // top_count
    slot_table = jnp.full((experts_total * capacity,), tok_rows, jnp.int32).at[target].set(sources)
    padded = jnp.concatenate([normed, jnp.zeros((1, model_width), jnp.bfloat16)], axis=0)
    outgoing = padded[slot_table].reshape(experts_total, capacity, model_width)
    answered = apply_expert(
        lax.all_to_all(outgoing, ("sp", "dp"), split_axis=0, concat_axis=0, tiled=True),
        expert_gate[0],
        expert_up[0],
        expert_down[0],
    )
    returned = lax.all_to_all(answered, ("sp", "dp"), split_axis=0, concat_axis=0, tiled=True)
    results = returned.reshape(experts_total * capacity, model_width)[target]
    weighted = results.astype(jnp.float32) * route_weight[0].reshape(-1)[:, None]
    combined = jnp.sum(weighted.reshape(tok_rows, top_count, model_width), axis=1)
    return (widened + combined).astype(jnp.bfloat16)[None]


def solution(mesh):
    placed = (
        P("dp", "sp", None),
        P("dp", "sp", None),
        P("dp", "sp", None),
        P("dp", "sp", None),
        P(),
        P(),
        P("dp", None),
        P(),
        P("dp", "sp", None),
        P("dp", "sp", None),
        P(("sp", "dp"), None, None),
        P(("sp", "dp"), None, None),
        P(("sp", "dp"), None, None),
    )
    return jax.shard_map(
        per_device, mesh=mesh, in_specs=placed, out_specs=P("dp", "sp", None), check_vma=False
    )
```

profile of v0, /device:TPU:0, one launch (start us, length us, event | category | flops | bytes accessed | tf_op | source)
XLA Modules:
  0.0 339.7 jit_solution(17231066613141276203)
XLA Ops:
  7.3 1.1 reshape.295
  8.8 1.0 multiply_multiply_fusion
  9.8 0.9 subtract_convert_fusion.1
  10.7 0.8 pad_maximum_fusion.1
  11.6 0.9 broadcast_in_dim.16
  12.4 7.3 %all-to-all-start.1 = ((bf16[256,8,128]{2,0,1:T(8,128)(2,1)}), bf16[256,8,128]{2,0,1:T(8,128)(2,1)S(1)}, u32[]{:S(2)}, u32[]{:S(2)}) async-start(bf16[256,8,128]{2,0,1:T(8,128)(2,1)} %bitcast.22), calls=%async_computation.1 | async-start | bytes 1048576 | tf_op jit(solution)/shard_map/all_to_all | solution.py:111
  19.7 0.5 copy.111
  21.2 1.0 pad_maximum_fusion
  22.3 11.9 %all-to-all-done.1 = bf16[256,8,128]{2,0,1:T(8,128)(2,1)S(1)} async-done(((bf16[256,8,128]{2,0,1:T(8,128)(2,1)}), bf16[256,8,128]{2,0,1:T(8,128)(2,1)S(1)}, u32[]{:S(2)}, u32[]{:S(2)}) %all-to-all-start.1) | async-done | bytes 524320 | tf_op jit(solution)/shard_map/all_to_all | solution.py:111
  34.2 3.6 %all-to-all-start = ((bf16[256,16,128]{0,2,1:T(8,128)(2,1)}), bf16[256,16,128]{0,2,1:T(8,128)(2,1)S(1)}, u32[]{:S(2)}, u32[]{:S(2)}) async-start(bf16[256,16,128]{0,2,1:T(8,128)(2,1)} %pad_maximum_fusion), calls=%async_computation | async-start | bytes 2097152 | tf_op jit(solution)/shard_map/all_to_all | solution.py:110
  37.9 0.7 all-gather.2.cloned.1.call-update
  38.7 25.1 %all-to-all-done = bf16[256,16,128]{0,2,1:T(8,128)(2,1)S(1)} async-done(((bf16[256,16,128]{0,2,1:T(8,128)(2,1)}), bf16[256,16,128]{0,2,1:T(8,128)(2,1)S(1)}, u32[]{:S(2)}, u32[]{:S(2)}) %all-to-all-start) | async-done | bytes 1048608 | tf_op jit(solution)/shard_map/all_to_all | solution.py:110
  63.8 0.9 broadcast_in_dim.17
  64.7 3.6 %all-to-all-start.2 = ((bf16[256,8,128]{2,0,1:T(8,128)(2,1)}), bf16[256,8,128]{2,0,1:T(8,128)(2,1)S(1)}, u32[]{:S(2)}, u32[]{:S(2)}) async-start(bf16[256,8,128]{2,0,1:T(8,128)(2,1)} %bitcast.26), calls=%async_computation.2 | async-start | bytes 1048576 | tf_op jit(solution)/shard_map/all_to_all | solution.py:112
  68.3 0.7 copy.113
  69.0 14.0 %all-to-all-done.2 = bf16[256,8,128]{2,0,1:T(8,128)(2,1)S(1)} async-done(((bf16[256,8,128]{2,0,1:T(8,128)(2,1)}), bf16[256,8,128]{2,0,1:T(8,128)(2,1)S(1)}, u32[]{:S(2)}, u32[]{:S(2)}) %all-to-all-start.2) | async-done | bytes 524320 | tf_op jit(solution)/shard_map/all_to_all | solution.py:112
  83.0 22.7 %while.10 = (s32[]{:T(128)}, bf16[4,512,1,2,128]{4,1,0,3,2:T(8,128)(2,1)}, bf16[4,512,1,2,128]{4,1,0,3,2:T(8,128)(2,1)S(1)}, bf16[2048,1,128]{2,0,1:T(8,128)(2,1...) while((s32[]{:T(128)}, bf16[4,512,1,2,128]{4,1,0,3,2:T(8,128)(2,1)}, ...), condition=%wide.region_5.6_spmd, body=%wide.region_2.5_spmd.sunk | while | flops 1092745216 | bytes 26759752 | solution.py:65
  83.0 1.3 bitcast_reduce_fusion.2
  84.3 1.6 fusion.63
  86.0 2.7 fusion.64
  88.7 1.3 bitcast_reduce_fusion.2
  90.0 1.6 fusion.63
  91.7 2.7 fusion.64
  94.4 1.3 bitcast_reduce_fusion.2
  95.7 1.6 fusion.63
  97.3 2.7 fusion.64
  100.0 1.3 bitcast_reduce_fusion.2
  101.4 1.6 fusion.63
  103.0 2.7 fusion.64
  105.7 3.7 %copy.124 = bf16[2048,2,128]{2,1,0:T(2,128)(2,1)} copy(bf16[2048,2,128]{2,0,1:T(8,128)(2,1)} %bitcast.160) | data formatting | bytes 2097152 | tf_op jit(solution)/shard_map/reshape | solution.py:65
  109.4 3.6 %all-to-all-start.3 = ((bf16[2048,2,128]{2,1,0:T(2,128)(2,1)}), bf16[2048,2,128]{2,1,0:T(2,128)(2,1)S(1)}, u32[]{:S(2)}, u32[]{:S(2)}) async-start(bf16[2048,2,128]{2,1,0:T(2,128)(2,1)} %copy.124), calls=%async_computation.3 | async-start | bytes 2097152 | tf_op jit(solution)/shard_map/all_to_all | solution.py:115
  113.5 1.2 reduce-window.6
  115.4 2.6 scatter_custom_fusion
  118.0 21.0 %all-to-all-done.3 = bf16[2048,2,128]{2,1,0:T(2,128)(2,1)S(1)} async-done(((bf16[2048,2,128]{2,1,0:T(2,128)(2,1)}), bf16[2048,2,128]{2,1,0:T(2,128)(2,1)S(1)}, u32[]{:S(2)}, u32[]{:S(2)}) %all-to-all-start.3) | async-done | bytes 1048608 | tf_op jit(solution)/shard_map/all_to_all | solution.py:115
  139.1 0.5 copy.126
  139.7 5.9 %fusion.33 = (f32[256]{0:T(256)S(1)}, bf16[256,2048]{1,0:T(8,128)(2,1)S(1)}) fusion(bf16[256,2048]{0,1:T(8,128)(2,1)S(1)} %bitcast.153, bf16[2048,2048]{1,0:T(8,128)(2,1)} %all-gather.2.cloned.1.call-done, bf16[1,256,2048]{2,1,0:T(8,128)(2,1)S(1)} %copy-done.2), kind=kOutput, calls=%fused_computation.39 | convolution fusion | flops 2150629120 | bytes 11535360 | tf_op jit(solution)/shard_map/dot_general | solution.py:118
  145.6 1.0 copy-done
  147.0 4.3 %gather_fusion = bf16[768,2048]{1,0:T(8,128)(2,1)} fusion(bf16[257,2048]{1,0:T(8,128)(2,1)S(1)} %concatenate.13, s32[1024]{0:T(1024)S(1)} %pad_clamp_fusion.1), kind=kCustom, calls=%fused_computation | custom fusion | bytes 6294528 | tf_op jit(solution)/shard_map/gather | solution.py:141
  151.3 74.8 %all_to_all.76 = bf16[32,24,2048]{2,1,0:T(8,128)(2,1)S(1)} all-to-all(bf16[32,24,2048]{2,1,0:T(8,128)(2,1)} %bitcast.150), channel_id=1, replica_groups=mesh['sp'=8,'dp'=4] {'sp','dp'}, dimensions={0} | all-to-all | bytes 6291456 | tf_op jit(solution)/shard_map/all_to_all | solution.py:143
  226.1 3.4 %fusion.23 = f32[768,1024]{1,0:T(8,128)S(1)} fusion(bf16[768,2048]{1,0:T(8,128)(2,1)S(1)} %bitcast.158, bf16[1,2048,1024]{2,1,0:T(8,128)(2,1)S(1)} %copy-done.9), kind=kOutput, calls=%fused_computation.23 | convolution fusion | flops 3221225472 | bytes 10485760 | tf_op jit(solution)/shard_map/dot_general | solution.py:72
  229.6 4.1 %multiply_convert_fusion = bf16[768,1024]{1,0:T(8,128)(2,1)S(1)} fusion(f32[768,1024]{1,0:T(8,128)S(1)} %fusion.23, bf16[768,2048]{1,0:T(8,128)(2,1)S(1)} %bitcast.159, bf16[1,2048,1024]{2,1,0:T(8,128)(2,1)S(1)} %copy-done.10), kind=kOutput, calls=%fused_computation.29 | convolution fusion | flops 3229089792 | bytes 12058624 | tf_op jit(solution)/shard_map/dot_general | solution.py:70
  233.7 4.8 %fusion.27 = bf16[768,2048]{1,0:T(8,128)(2,1)} fusion(bf16[768,1024]{1,0:T(8,128)(2,1)S(1)} %multiply_convert_fusion, bf16[1,1024,2048]{2,1,0:T(8,128)(2,1)S(1)} %copy-done.11), kind=kOutput, calls=%fused_computation.28 | convolution fusion | flops 3222798336 | bytes 8912896 | tf_op jit(solution)/shard_map/dot_general | solution.py:76
  238.5 3.9 %all-to-all-start.5 = ((bf16[32,24,2048]{2,1,0:T(8,128)(2,1)}), bf16[32,24,2048]{2,1,0:T(8,128)(2,1)S(1)}, u32[]{:S(2)}, u32[]{:S(2)}) async-start(bf16[32,24,2048]{2,1,0:T(8,128)(2,1)} %bitcast.157), calls=%async_computation.5 | async-start | bytes 6291456 | tf_op jit(solution)/shard_map/all_to_all | solution.py:148
  242.6 71.2 %all-to-all-done.5 = bf16[32,24,2048]{2,1,0:T(8,128)(2,1)S(1)} async-done(((bf16[32,24,2048]{2,1,0:T(8,128)(2,1)}), bf16[32,24,2048]{2,1,0:T(8,128)(2,1)S(1)}, u32[]{:S(2)}, u32[]{:S(2)}) %all-to-all-start.5) | async-done | bytes 3145760 | tf_op jit(solution)/shard_map/all_to_all | solution.py:148
  313.8 3.3 gather_fusion.1
  317.1 5.4 %reshape.296 = f32[256,2,2048]{2,1,0:T(2,128)} reshape(bf16[512,2048]{1,0:T(8,128)(2,1)} %gather_fusion.1) | data formatting | bytes 6291456 | tf_op jit(solution)/shard_map/convert_element_type | solution.py:150
  322.6 9.0 %multiply_reduce_fusion = f32[256,2048]{1,0:T(8,128)S(1)} fusion(f32[256,2,2048]{2,1,0:T(2,128)} %reshape.296, f32[256,2]{1,0:T(8,128)S(1)} %copy.131), kind=kLoop, calls=%fused_computation.27 | loop fusion | flops 1572864 | bytes 6293504 | tf_op jit(solution)/shard_map/reduce_sum | solution.py:151
  331.5 1.3 fusion.39
  (63 shorter events, 4.0 us)
Async XLA Ops:
  9.8 9.9 %copy-start.3 = (bf16[1,256,2048]{2,1,0:T(8,128)(2,1)S(1)}, bf16[1,256,2048]{2,1,0:T(8,128)(2,1)}, u32[]{:S(2)}) copy-start(bf16[1,256,2048]{2,1,0:T(8,128)(2,1)} %param.16) | copy-start | bytes 3145732
  10.7 9.8 %copy-start.8 = (f32[128]{0:T(128)S(1)}, f32[128]{0:T(128)}, u32[]{:S(2)}) copy-start(f32[128]{0:T(128)} %param.19) | copy-start | bytes 1540
  12.4 21.8 %all-to-all-start.1 = ((bf16[256,8,128]{2,0,1:T(8,128)(2,1)}), bf16[256,8,128]{2,0,1:T(8,128)(2,1)S(1)}, u32[]{:S(2)}, u32[]{:S(2)}) async-start(bf16[256,8,128]{2,0,1:T(8,128)(2,1)} %bitcast.22), calls=%async_computation.1 | async-start | bytes 1048576 | tf_op jit(solution)/shard_map/all_to_all | solution.py:111
  21.2 17.3 %copy-start.4 = (bf16[1,256,512]{2,1,0:T(8,128)(2,1)S(1)}, bf16[1,256,512]{2,1,0:T(8,128)(2,1)}, u32[]{:S(2)}) copy-start(bf16[1,256,512]{2,1,0:T(8,128)(2,1)} %param.18) | copy-start | bytes 786436
  34.2 29.6 %all-to-all-start = ((bf16[256,16,128]{0,2,1:T(8,128)(2,1)}), bf16[256,16,128]{0,2,1:T(8,128)(2,1)S(1)}, u32[]{:S(2)}, u32[]{:S(2)}) async-start(bf16[256,16,128]{0,2,1:T(8,128)(2,1)} %pad_maximum_fusion), calls=%async_computation | async-start | bytes 2097152 | tf_op jit(solution)/shard_map/all_to_all | solution.py:110
  37.8 101.9 %all-gather.2.cloned.1.call-start = ((), (), s32[]{:S(2)}) async-start(), calls=%async_computation.6 | async-start | bytes 10485760 | tf_op jit(solution)/shard_map/all_gather | solution.py:120
  64.7 18.3 %all-to-all-start.2 = ((bf16[256,8,128]{2,0,1:T(8,128)(2,1)}), bf16[256,8,128]{2,0,1:T(8,128)(2,1)S(1)}, u32[]{:S(2)}, u32[]{:S(2)}) async-start(bf16[256,8,128]{2,0,1:T(8,128)(2,1)} %bitcast.26), calls=%async_computation.2 | async-start | bytes 1048576 | tf_op jit(solution)/shard_map/all_to_all | solution.py:112
  105.7 7.3 %copy-start.6 = (s32[1,256,2]{1,2,0:T(2,128)S(1)}, s32[1,256,2]{1,2,0:T(2,128)}, u32[]{:S(2)}) copy-start(s32[1,256,2]{1,2,0:T(2,128)} %param.23) | copy-start | bytes 6148
  109.4 29.6 %all-to-all-start.3 = ((bf16[2048,2,128]{2,1,0:T(2,128)(2,1)}), bf16[2048,2,128]{2,1,0:T(2,128)(2,1)S(1)}, u32[]{:S(2)}, u32[]{:S(2)}) async-start(bf16[2048,2,128]{2,1,0:T(2,128)(2,1)} %copy.124), calls=%async_computation.3 | async-start | bytes 2097152 | tf_op jit(solution)/shard_map/all_to_all | solution.py:115
  113.0 26.7 %copy-start.2 = (bf16[1,256,2048]{2,1,0:T(8,128)(2,1)S(1)}, bf16[1,256,2048]{2,1,0:T(8,128)(2,1)}, u32[]{:S(2)}) copy-start(bf16[1,256,2048]{2,1,0:T(8,128)(2,1)} %param.15) | copy-start | bytes 3145732
  139.7 6.9 %copy-start.5 = (f32[2048]{0:T(1024)S(1)}, f32[2048]{0:T(1024)}, u32[]{:S(2)}) copy-start(f32[2048]{0:T(1024)} %param.22) | copy-start | bytes 24580
  145.6 1.0 copy-start
  151.3 74.8 %copy-start.9 = (bf16[1,2048,1024]{2,1,0:T(8,128)(2,1)S(1)}, bf16[1,2048,1024]{2,1,0:T(8,128)(2,1)}, u32[]{:S(2)}) copy-start(bf16[1,2048,1024]{2,1,0:T(8,128)(2,1)} %param.26) | copy-start | bytes 12582916
  226.1 3.5 %copy-start.10 = (bf16[1,2048,1024]{2,1,0:T(8,128)(2,1)S(1)}, bf16[1,2048,1024]{2,1,0:T(8,128)(2,1)}, u32[]{:S(2)}) copy-start(bf16[1,2048,1024]{2,1,0:T(8,128)(2,1)} %param.25) | copy-start | bytes 12582916
  229.6 4.2 %copy-start.11 = (bf16[1,1024,2048]{2,1,0:T(8,128)(2,1)S(1)}, bf16[1,1024,2048]{2,1,0:T(8,128)(2,1)}, u32[]{:S(2)}) copy-start(bf16[1,1024,2048]{2,1,0:T(8,128)(2,1)} %param.27) | copy-start | bytes 12582916
  238.5 3.9 %copy-start.7 = (f32[1,256,2]{1,2,0:T(2,128)S(1)}, f32[1,256,2]{1,2,0:T(2,128)}, u32[]{:S(2)}) copy-start(f32[1,256,2]{1,2,0:T(2,128)} %param.24) | copy-start | bytes 6148
  238.5 75.3 %all-to-all-start.5 = ((bf16[32,24,2048]{2,1,0:T(8,128)(2,1)}), bf16[32,24,2048]{2,1,0:T(8,128)(2,1)S(1)}, u32[]{:S(2)}, u32[]{:S(2)}) async-start(bf16[32,24,2048]{2,1,0:T(8,128)(2,1)} %bitcast.157), calls=%async_computation.5 | async-start | bytes 6291456 | tf_op jit(solution)/shard_map/all_to_all | solution.py:148
  322.6 9.0 %copy-start.1 = (bf16[256,2048]{1,0:T(8,128)(2,1)S(1)}, bf16[256,2048]{1,0:T(8,128)(2,1)}, u32[]{:S(2)}) copy-start(bf16[256,2048]{1,0:T(8,128)(2,1)} %copy-done) | copy-start | bytes 3145732
Sparse Core Ops, SparseCore 0:
  40.2 59.6 all-gather.1
where the time goes:
time: 340 us
  waiting for transfers between devices  144 us (42%)
  blocking collectives  74.8 us (22%)
  matrix products  34.4 us (10%)
  local copies, waits for them, and re-layouts  26.8 us (8%)
  other arithmetic  23.8 us (7%)
  starting transfers between devices  22.1 us (6%)
  between operations  13.8 us (4%)
    all_to_all x1, blocking collectives, per_device(): lax.all_to_all(outgoing, ('sp', 'dp'), split_axis=0, concat_axis=0, tiled...  74.8 us
    all_to_all x1, waiting for transfers between devices, per_device(): lax.all_to_all(answered, ('sp', 'dp'), split_axis=0, concat_axis=0, tiled...  71.2 us
    all_to_all x1, waiting for transfers between devices, per_device(): lax.all_to_all(query_turned, 'sp', split_axis=1, concat_axis=0, tiled=True)  25.1 us
    all_to_all x1, waiting for transfers between devices, per_device(): lax.all_to_all(head_out, 'sp', split_axis=0, concat_axis=1, tiled=True)  21 us
    all_to_all x1, waiting for transfers between devices, per_device(): lax.all_to_all(value_heads, 'sp', split_axis=1, concat_axis=0, tiled=True)  14 us
    all_to_all x1, waiting for transfers between devices, per_device(): lax.all_to_all(key_turned, 'sp', split_axis=1, concat_axis=0, tiled=True)  11.9 us
    dot_general x4, matrix products, one_block(): jnp.einsum('kgqs,skd->qkgd', attn_weights, head_value, preferred_element_...  10.8 us
    reduce_sum x1, other arithmetic, per_device(): jnp.sum(weighted.reshape(tok_rows, top_count, model_width), axis=1)  8.96 us
  transfers between devices with their start and end apart: 6, of which 5 were waited for; matrix products, arithmetic and copies ran while one was open for 11% of the time, Pallas kernels for 0%

commit v1 on v0

--- a/solution.py
+++ b/solution.py
@@ -108,7 +108,12 @@
     value_heads = jnp.repeat(values[0].reshape(tok_rows, kv_heads, head_dim), repeat_count, axis=1)
     head_query, head_key, head_value = (
         lax.all_to_all(query_turned, "sp", split_axis=1, concat_axis=0, tiled=True),
-        lax.all_to_all(key_turned, "sp", split_axis=1, concat_axis=0, tiled=True),
+        jnp.concatenate(
+            lax.all_to_all(
+                jnp.stack(jnp.split(key_turned, lax.axis_size("sp"), axis=1)), "sp", 0, 0
+            ),
+            axis=0,
+        ),
         lax.all_to_all(value_heads, "sp", split_axis=1, concat_axis=0, tiled=True),
     )
     head_out = attend(head_query, head_key, head_value)

time: 340 us -> 345 us (1.015)
  local copies, waits for them, and re-layouts: 26.8 us -> 31 us
    unnamed x26 -> x33, local copies, waits for them, and re-layouts: 1.67 us -> 6.06 us
where the time goes in v1:
time: 345 us; the launch traced here: 344 us
  waiting for transfers between devices  144 us (42%)
  blocking collectives  74.8 us (22%)
  matrix products  34.4 us (10%)
  local copies, waits for them, and re-layouts  31 us (9%)
  other arithmetic  23.8 us (7%)
  starting transfers between devices  22.1 us (6%)
  between operations  13.8 us (4%)
    all_to_all x1, blocking collectives, per_device(): lax.all_to_all(outgoing, ('sp', 'dp'), split_axis=0, concat_axis=0, tiled...  74.8 us
    all_to_all x1, waiting for transfers between devices, per_device(): lax.all_to_all(answered, ('sp', 'dp'), split_axis=0, concat_axis=0, tiled...  71.2 us
    all_to_all x1, waiting for transfers between devices, per_device(): lax.all_to_all(query_turned, 'sp', split_axis=1, concat_axis=0, tiled=True)  25.1 us
    all_to_all x1, waiting for transfers between devices, per_device(): lax.all_to_all(head_out, 'sp', split_axis=0, concat_axis=1, tiled=True)  21 us
    all_to_all x1, waiting for transfers between devices, per_device(): lax.all_to_all(value_heads, 'sp', split_axis=1, concat_axis=0, tiled=True)  14 us
    all_to_all x1, waiting for transfers between devices, per_device(): lax.all_to_all(jnp.stack(jnp.split(key_turned, lax.axis_size('sp'), axis=...  11.9 us
    dot_general x4, matrix products, one_block(): jnp.einsum('kgqs,skd->qkgd', attn_weights, head_value, preferred_element_...  10.8 us
    reduce_sum x1, other arithmetic, per_device(): jnp.sum(weighted.reshape(tok_rows, top_count, model_width), axis=1)  8.96 us
  transfers between devices with their start and end apart: 6, of which 5 were waited for; matrix products, arithmetic and copies ran while one was open for 11% of the time, Pallas kernels for 0%

profile of v1, /device:TPU:0, one launch (start us, length us, event | category | flops | bytes accessed | tf_op | source)
XLA Modules:
  0.0 343.9 jit_solution(8889461181076416127)
XLA Ops:
  7.3 1.1 reshape.299
  8.8 1.0 multiply_multiply_fusion
  9.8 0.9 subtract_convert_fusion.1
  10.7 0.8 pad_maximum_fusion.1
  12.9 0.6 fusion.48
  13.5 0.6 fusion.47
  16.0 0.6 fusion.43
  16.7 7.3 %all-to-all-start.1 = ((bf16[8,256,1,128]{3,1,2,0:T(8,128)(2,1)}), bf16[8,256,1,128]{3,1,2,0:T(8,128)(2,1)S(1)}, u32[]{:S(2)}, u32[]{:S(2)}) async-start(bf16[8,256,1,128]{3,1,2,0:T(8,128)(2,1)} %fusion.43), calls=%async_computation.1 | async-start | bytes 1048576 | tf_op jit(solution)/shard_map/all_to_all | solution.py:112
  25.5 1.0 pad_maximum_fusion
  26.5 11.9 %all-to-all-done.1 = bf16[8,256,1,128]{3,1,2,0:T(8,128)(2,1)S(1)} async-done(((bf16[8,256,1,128]{3,1,2,0:T(8,128)(2,1)}), bf16[8,256,1,128]{3,1,2,0:T(8,128)(2,1)S(1)}, u32[]{:S(2)}, u32[]{:S(2)}) %all-to-all-start.1) | async-done | bytes 524320 | tf_op jit(solution)/shard_map/all_to_all | solution.py:112
  38.4 3.6 %all-to-all-start = ((bf16[256,16,128]{0,2,1:T(8,128)(2,1)}), bf16[256,16,128]{0,2,1:T(8,128)(2,1)S(1)}, u32[]{:S(2)}, u32[]{:S(2)}) async-start(bf16[256,16,128]{0,2,1:T(8,128)(2,1)} %pad_maximum_fusion), calls=%async_computation | async-start | bytes 2097152 | tf_op jit(solution)/shard_map/all_to_all | solution.py:110
  42.1 0.7 all-gather.2.cloned.1.call-update
  42.9 25.1 %all-to-all-done = bf16[256,16,128]{0,2,1:T(8,128)(2,1)S(1)} async-done(((bf16[256,16,128]{0,2,1:T(8,128)(2,1)}), bf16[256,16,128]{0,2,1:T(8,128)(2,1)S(1)}, u32[]{:S(2)}, u32[]{:S(2)}) %all-to-all-start) | async-done | bytes 1048608 | tf_op jit(solution)/shard_map/all_to_all | solution.py:110
  68.0 0.9 broadcast_in_dim.17
  68.9 3.6 %all-to-all-start.2 = ((bf16[256,8,128]{2,0,1:T(8,128)(2,1)}), bf16[256,8,128]{2,0,1:T(8,128)(2,1)S(1)}, u32[]{:S(2)}, u32[]{:S(2)}) async-start(bf16[256,8,128]{2,0,1:T(8,128)(2,1)} %bitcast.32), calls=%async_computation.2 | async-start | bytes 1048576 | tf_op jit(solution)/shard_map/all_to_all | solution.py:117
  72.6 0.7 copy.141
  73.3 14.0 %all-to-all-done.2 = bf16[256,8,128]{2,0,1:T(8,128)(2,1)S(1)} async-done(((bf16[256,8,128]{2,0,1:T(8,128)(2,1)}), bf16[256,8,128]{2,0,1:T(8,128)(2,1)S(1)}, u32[]{:S(2)}, u32[]{:S(2)}) %all-to-all-start.2) | async-done | bytes 524320 | tf_op jit(solution)/shard_map/all_to_all | solution.py:117
  87.3 22.7 %while.10 = (s32[]{:T(128)}, bf16[4,512,1,2,128]{4,1,0,3,2:T(8,128)(2,1)}, bf16[4,512,1,2,128]{4,1,0,3,2:T(8,128)(2,1)S(1)}, bf16[2048,1,128]{2,0,1:T(8,128)(2,1...) while((s32[]{:T(128)}, bf16[4,512,1,2,128]{4,1,0,3,2:T(8,128)(2,1)}, ...), condition=%wide.region_5.6_spmd, body=%wide.region_2.5_spmd.sunk | while | flops 1092745216 | bytes 26759752 | solution.py:65
  87.3 1.3 bitcast_reduce_fusion.2
  88.6 1.6 fusion.71
  90.2 2.7 fusion.72
  92.9 1.3 bitcast_reduce_fusion.2
  94.3 1.6 fusion.71
  95.9 2.7 fusion.72
  98.6 1.3 bitcast_reduce_fusion.2
  99.9 1.6 fusion.71
  101.6 2.7 fusion.72
  104.3 1.3 bitcast_reduce_fusion.2
  105.6 1.6 fusion.71
  107.3 2.7 fusion.72
  110.0 3.7 %copy.152 = bf16[2048,2,128]{2,1,0:T(2,128)(2,1)} copy(bf16[2048,2,128]{2,0,1:T(8,128)(2,1)} %bitcast.196) | data formatting | bytes 2097152 | tf_op jit(solution)/shard_map/reshape | solution.py:65
  113.7 3.6 %all-to-all-start.3 = ((bf16[2048,2,128]{2,1,0:T(2,128)(2,1)}), bf16[2048,2,128]{2,1,0:T(2,128)(2,1)S(1)}, u32[]{:S(2)}, u32[]{:S(2)}) async-start(bf16[2048,2,128]{2,1,0:T(2,128)(2,1)} %copy.152), calls=%async_computation.3 | async-start | bytes 2097152 | tf_op jit(solution)/shard_map/all_to_all | solution.py:120
  117.7 1.2 reduce-window.6
  119.6 2.6 scatter_custom_fusion
  122.3 21.0 %all-to-all-done.3 = bf16[2048,2,128]{2,1,0:T(2,128)(2,1)S(1)} async-done(((bf16[2048,2,128]{2,1,0:T(2,128)(2,1)}), bf16[2048,2,128]{2,1,0:T(2,128)(2,1)S(1)}, u32[]{:S(2)}, u32[]{:S(2)}) %all-to-all-start.3) | async-done | bytes 1048608 | tf_op jit(solution)/shard_map/all_to_all | solution.py:120
  144.0 5.9 %fusion.33 = (f32[256]{0:T(256)S(1)}, bf16[256,2048]{1,0:T(8,128)(2,1)S(1)}) fusion(bf16[256,2048]{0,1:T(8,128)(2,1)S(1)} %bitcast.181, bf16[2048,2048]{1,0:T(8,128)(2,1)} %all-gather.2.cloned.1.call-done, bf16[1,256,2048]{2,1,0:T(8,128)(2,1)S(1)} %copy-done.2), kind=kOutput, calls=%fused_computation.39 | convolution fusion | flops 2150629120 | bytes 11535360 | tf_op jit(solution)/shard_map/dot_general | solution.py:123
  149.9 1.0 copy-done
  151.2 4.3 %gather_fusion = bf16[768,2048]{1,0:T(8,128)(2,1)} fusion(bf16[257,2048]{1,0:T(8,128)(2,1)S(1)} %concatenate.13, s32[1024]{0:T(1024)S(1)} %pad_clamp_fusion.1), kind=kCustom, calls=%fused_computation | custom fusion | bytes 6294528 | tf_op jit(solution)/shard_map/gather | solution.py:146
  155.5 74.8 %all_to_all.63 = bf16[32,24,2048]{2,1,0:T(8,128)(2,1)S(1)} all-to-all(bf16[32,24,2048]{2,1,0:T(8,128)(2,1)} %bitcast.178), channel_id=1, replica_groups=mesh['sp'=8,'dp'=4] {'sp','dp'}, dimensions={0} | all-to-all | bytes 6291456 | tf_op jit(solution)/shard_map/all_to_all | solution.py:148
  230.3 3.4 %fusion.23 = f32[768,1024]{1,0:T(8,128)S(1)} fusion(bf16[768,2048]{1,0:T(8,128)(2,1)S(1)} %bitcast.186, bf16[1,2048,1024]{2,1,0:T(8,128)(2,1)S(1)} %copy-done.9), kind=kOutput, calls=%fused_computation.23 | convolution fusion | flops 3221225472 | bytes 10485760 | tf_op jit(solution)/shard_map/dot_general | solution.py:72
  233.8 4.1 %multiply_convert_fusion = bf16[768,1024]{1,0:T(8,128)(2,1)S(1)} fusion(f32[768,1024]{1,0:T(8,128)S(1)} %fusion.23, bf16[768,2048]{1,0:T(8,128)(2,1)S(1)} %bitcast.187, bf16[1,2048,1024]{2,1,0:T(8,128)(2,1)S(1)} %copy-done.10), kind=kOutput, calls=%fused_computation.29 | convolution fusion | flops 3229089792 | bytes 12058624 | tf_op jit(solution)/shard_map/dot_general | solution.py:70
  238.0 4.8 %fusion.27 = bf16[768,2048]{1,0:T(8,128)(2,1)} fusion(bf16[768,1024]{1,0:T(8,128)(2,1)S(1)} %multiply_convert_fusion, bf16[1,1024,2048]{2,1,0:T(8,128)(2,1)S(1)} %copy-done.11), kind=kOutput, calls=%fused_computation.28 | convolution fusion | flops 3222798336 | bytes 8912896 | tf_op jit(solution)/shard_map/dot_general | solution.py:76
  242.8 3.9 %all-to-all-start.5 = ((bf16[32,24,2048]{2,1,0:T(8,128)(2,1)}), bf16[32,24,2048]{2,1,0:T(8,128)(2,1)S(1)}, u32[]{:S(2)}, u32[]{:S(2)}) async-start(bf16[32,24,2048]{2,1,0:T(8,128)(2,1)} %bitcast.185), calls=%async_computation.5 | async-start | bytes 6291456 | tf_op jit(solution)/shard_map/all_to_all | solution.py:153
  246.8 71.2 %all-to-all-done.5 = bf16[32,24,2048]{2,1,0:T(8,128)(2,1)S(1)} async-done(((bf16[32,24,2048]{2,1,0:T(8,128)(2,1)}), bf16[32,24,2048]{2,1,0:T(8,128)(2,1)S(1)}, u32[]{:S(2)}, u32[]{:S(2)}) %all-to-all-start.5) | async-done | bytes 3145760 | tf_op jit(solution)/shard_map/all_to_all | solution.py:153
  318.0 3.3 gather_fusion.1
  321.4 5.4 %reshape.300 = f32[256,2,2048]{2,1,0:T(2,128)} reshape(bf16[512,2048]{1,0:T(8,128)(2,1)} %gather_fusion.1) | data formatting | bytes 6291456 | tf_op jit(solution)/shard_map/convert_element_type | solution.py:155
  326.8 9.0 %multiply_reduce_fusion = f32[256,2048]{1,0:T(8,128)S(1)} fusion(f32[256,2,2048]{2,1,0:T(2,128)} %reshape.300, f32[256,2]{1,0:T(8,128)S(1)} %copy.159), kind=kLoop, calls=%fused_computation.27 | loop fusion | flops 1572864 | bytes 6293504 | tf_op jit(solution)/shard_map/reduce_sum | solution.py:156
  335.8 1.3 fusion.39
  (71 shorter events, 8.3 us)
Async XLA Ops:
  10.7 13.3 %copy-start.3 = (bf16[1,256,2048]{2,1,0:T(8,128)(2,1)S(1)}, bf16[1,256,2048]{2,1,0:T(8,128)(2,1)}, u32[]{:S(2)}) copy-start(bf16[1,256,2048]{2,1,0:T(8,128)(2,1)} %param.16) | copy-start | bytes 3145732
  11.6 13.2 %copy-start.8 = (f32[128]{0:T(128)S(1)}, f32[128]{0:T(128)}, u32[]{:S(2)}) copy-start(f32[128]{0:T(128)} %param.19) | copy-start | bytes 1540
  16.7 21.8 %all-to-all-start.1 = ((bf16[8,256,1,128]{3,1,2,0:T(8,128)(2,1)}), bf16[8,256,1,128]{3,1,2,0:T(8,128)(2,1)S(1)}, u32[]{:S(2)}, u32[]{:S(2)}) async-start(bf16[8,256,1,128]{3,1,2,0:T(8,128)(2,1)} %fusion.43), calls=%async_computation.1 | async-start | bytes 1048576 | tf_op jit(solution)/shard_map/all_to_all | solution.py:112
  25.5 17.3 %copy-start.4 = (bf16[1,256,512]{2,1,0:T(8,128)(2,1)S(1)}, bf16[1,256,512]{2,1,0:T(8,128)(2,1)}, u32[]{:S(2)}) copy-start(bf16[1,256,512]{2,1,0:T(8,128)(2,1)} %param.18) | copy-start | bytes 786436
  38.4 29.6 %all-to-all-start = ((bf16[256,16,128]{0,2,1:T(8,128)(2,1)}), bf16[256,16,128]{0,2,1:T(8,128)(2,1)S(1)}, u32[]{:S(2)}, u32[]{:S(2)}) async-start(bf16[256,16,128]{0,2,1:T(8,128)(2,1)} %pad_maximum_fusion), calls=%async_computation | async-start | bytes 2097152 | tf_op jit(solution)/shard_map/all_to_all | solution.py:110
  42.1 101.8 %all-gather.2.cloned.1.call-start = ((), (), s32[]{:S(2)}) async-start(), calls=%async_computation.6 | async-start | bytes 10485760 | tf_op jit(solution)/shard_map/all_gather | solution.py:125
  68.9 18.3 %all-to-all-start.2 = ((bf16[256,8,128]{2,0,1:T(8,128)(2,1)}), bf16[256,8,128]{2,0,1:T(8,128)(2,1)S(1)}, u32[]{:S(2)}, u32[]{:S(2)}) async-start(bf16[256,8,128]{2,0,1:T(8,128)(2,1)} %bitcast.32), calls=%async_computation.2 | async-start | bytes 1048576 | tf_op jit(solution)/shard_map/all_to_all | solution.py:117
  110.0 7.3 %copy-start.6 = (s32[1,256,2]{1,2,0:T(2,128)S(1)}, s32[1,256,2]{1,2,0:T(2,128)}, u32[]{:S(2)}) copy-start(s32[1,256,2]{1,2,0:T(2,128)} %param.23) | copy-start | bytes 6148
  113.7 29.6 %all-to-all-start.3 = ((bf16[2048,2,128]{2,1,0:T(2,128)(2,1)}), bf16[2048,2,128]{2,1,0:T(2,128)(2,1)S(1)}, u32[]{:S(2)}, u32[]{:S(2)}) async-start(bf16[2048,2,128]{2,1,0:T(2,128)(2,1)} %copy.152), calls=%async_computation.3 | async-start | bytes 2097152 | tf_op jit(solution)/shard_map/all_to_all | solution.py:120
  117.3 26.7 %copy-start.2 = (bf16[1,256,2048]{2,1,0:T(8,128)(2,1)S(1)}, bf16[1,256,2048]{2,1,0:T(8,128)(2,1)}, u32[]{:S(2)}) copy-start(bf16[1,256,2048]{2,1,0:T(8,128)(2,1)} %param.15) | copy-start | bytes 3145732
  143.9 6.9 %copy-start.5 = (f32[2048]{0:T(1024)S(1)}, f32[2048]{0:T(1024)}, u32[]{:S(2)}) copy-start(f32[2048]{0:T(1024)} %param.22) | copy-start | bytes 24580
  149.8 1.0 copy-start
  155.5 74.8 %copy-start.9 = (bf16[1,2048,1024]{2,1,0:T(8,128)(2,1)S(1)}, bf16[1,2048,1024]{2,1,0:T(8,128)(2,1)}, u32[]{:S(2)}) copy-start(bf16[1,2048,1024]{2,1,0:T(8,128)(2,1)} %param.26) | copy-start | bytes 12582916
  230.3 3.5 %copy-start.10 = (bf16[1,2048,1024]{2,1,0:T(8,128)(2,1)S(1)}, bf16[1,2048,1024]{2,1,0:T(8,128)(2,1)}, u32[]{:S(2)}) copy-start(bf16[1,2048,1024]{2,1,0:T(8,128)(2,1)} %param.25) | copy-start | bytes 12582916
  233.8 4.2 %copy-start.11 = (bf16[1,1024,2048]{2,1,0:T(8,128)(2,1)S(1)}, bf16[1,1024,2048]{2,1,0:T(8,128)(2,1)}, u32[]{:S(2)}) copy-start(bf16[1,1024,2048]{2,1,0:T(8,128)(2,1)} %param.27) | copy-start | bytes 12582916
  242.8 3.9 %copy-start.7 = (f32[1,256,2]{1,2,0:T(2,128)S(1)}, f32[1,256,2]{1,2,0:T(2,128)}, u32[]{:S(2)}) copy-start(f32[1,256,2]{1,2,0:T(2,128)} %param.24) | copy-start | bytes 6148
  242.8 75.3 %all-to-all-start.5 = ((bf16[32,24,2048]{2,1,0:T(8,128)(2,1)}), bf16[32,24,2048]{2,1,0:T(8,128)(2,1)S(1)}, u32[]{:S(2)}, u32[]{:S(2)}) async-start(bf16[32,24,2048]{2,1,0:T(8,128)(2,1)} %bitcast.185), calls=%async_computation.5 | async-start | bytes 6291456 | tf_op jit(solution)/shard_map/all_to_all | solution.py:153
  326.8 9.0 %copy-start.1 = (bf16[256,2048]{1,0:T(8,128)(2,1)S(1)}, bf16[256,2048]{1,0:T(8,128)(2,1)}, u32[]{:S(2)}) copy-start(bf16[256,2048]{1,0:T(8,128)(2,1)} %copy-done) | copy-start | bytes 3145732
Sparse Core Ops, SparseCore 0:
  44.4 59.6 all-gather.1
